TPU v7x, 32 devices: a whole 2x2x4 slice. The times are simulated.
32 devices in a mesh: kv: 8 (over z, y), tp: 4 (over x, core).
Axes of the slice: x: 2, y: 2, z: 4, core: 2. Of those that a mesh axis runs over, the one named last changes fastest.
Arguments:
- tokens: bfloat16 [4096, 2048], P('kv', 'tp'), may hold values from -9 to 9
- w_query: bfloat16 [2048, 1536], P(None, 'tp'), may hold values from -1 to 1
- w_key: bfloat16 [2048, 1536], P(None, 'tp'), may hold values from -1 to 1
- w_value: bfloat16 [2048, 1536], P(None, 'tp'), may hold values from -0.5 to 0.5
- w_out: bfloat16 [1536, 2048], P('tp'), may hold values from -0.15625 to 0.15625
- chosen: int32 [128, 24], P('kv'), may hold values from 0 to 127, as said below
Outputs:
- mixed: bfloat16 [4096, 2048], P(('kv', 'tp'))
Inputs may be any that keep to these rules, and one draw needn't show every extreme that they name: `chosen`: row c names blocks no later than c; its first entry is c and its second c - 1 (0 for row 0), and an entry may repeat. Taking the rows in aligned runs of 16, one run for each index of kv, the rows of one run name at most 2 distinct blocks lying in any one other index's positions; in every draw some index of kv names exactly 2 from every earlier index. Every run names some block of the index just before it and of the index half the axis before it, where those exist.
All inputs are finite; a program needn't handle non-finite values.
Results may differ from a plain program's by a relative error of at most 0.014.
Values may be sent and summed in bfloat16 or wider, within the bound.
A program may use at most 320 MiB of HBM per device.

v0:
```python
import jax
import jax.numpy as jnp
from jax import lax
from jax.sharding import PartitionSpec as P

HD = 128
BLK = 32
MOST = 2
NEG = -1e30


def attend(query_rows, key_rows, value_rows, block_ids, chosen, first_block):
    tok_rows, width = query_rows.shape
    head_count = width // HD
    key_count = key_rows.shape[0]
    slot_count = key_count // BLK
    query_blocks = tok_rows // BLK
    seen = (
        jnp.any(chosen[:, :, None] == block_ids[None, None, :], axis=1) & (block_ids >= 0)[None, :]
    )
    grid = jnp.broadcast_to(seen[:, None, :, None], (query_blocks, BLK, slot_count, BLK)).reshape(
        tok_rows, key_count
    )
    key_pos = (block_ids[:, None] * BLK + jnp.arange(BLK, dtype=jnp.int32)[None, :]).reshape(
        key_count
    )
    query_pos = first_block * BLK + jnp.arange(tok_rows, dtype=jnp.int32)
    allowed = grid & (key_pos[None, :] <= query_pos[:, None])
    query_heads = query_rows.reshape(tok_rows, head_count, HD)
    key_heads = key_rows.reshape(key_count, head_count, HD)
    value_heads = value_rows.reshape(key_count, head_count, HD)
    scores = jnp.einsum(
        "qhd,khd->hqk", query_heads, key_heads, preferred_element_type=jnp.float32
    ) * HD ** (-0.5)
    scores = jnp.where(allowed[None], scores, NEG)
    highest = jnp.max(scores, axis=-1)
    weights = jnp.where(allowed[None], jnp.exp(scores - highest[..., None]), 0.0)
    totals = jnp.sum(weights, axis=-1)
    summed = jnp.einsum("hqk,khd->hqd", weights, value_heads.astype(jnp.float32))
    return (highest, totals, summed)


def combine(left, right):
    highest = jnp.maximum(left[0], right[0])
    left_scale = jnp.exp(left[0] - highest)
    right_scale = jnp.exp(right[0] - highest)
    totals = left[1] * left_scale + right[1] * right_scale
    summed = left[2] * left_scale[..., None] + right[2] * right_scale[..., None]
    return (highest, totals, summed)


def local(tokens, w_query, w_key, w_value, w_out, chosen):
    tok_rows = tokens.shape[0]
    width = w_query.shape[1]
    empty = jnp.zeros((tok_rows, width), jnp.float32)
    totals = (empty, empty, empty)
    piece = lax.all_gather(tokens, "tp", axis=1, tiled=True)
    outputs = []
    for total, weight in zip(totals, (w_query, w_key, w_value)):
        rows = weight
        outputs.append(jnp.dot(piece, rows, preferred_element_type=jnp.float32))
    query_full, key_full, value_full = tuple(outputs)
    query_rows = query_full.astype(jnp.bfloat16)
    key_rows = key_full.astype(jnp.bfloat16)
    value_rows = value_full.astype(jnp.bfloat16)
    per_dev = tok_rows // BLK
    my_index = lax.axis_index("kv")
    first_block = my_index * per_dev
    own_ids = first_block + jnp.arange(per_dev, dtype=jnp.int32)
    own_part = attend(query_rows, key_rows, value_rows, own_ids, chosen, first_block)
    peers = lax.axis_size("kv")
    block_total = peers * per_dev
    wanted = jnp.any(
        chosen[:, :, None] == jnp.arange(block_total, dtype=jnp.int32)[None, None, :], axis=(0, 1)
    )
    peer_ids = jnp.arange(peers, dtype=jnp.int32)
    wanted = wanted.reshape(peers, per_dev) & (peer_ids != my_index)[:, None]
    ranks = jnp.cumsum(wanted.astype(jnp.int32), axis=1) - 1
    slot_hit = wanted[:, :, None] & (
        ranks[:, :, None] == jnp.arange(MOST, dtype=jnp.int32)[None, None, :]
    )
    local_ids = jnp.sum(
        slot_hit.astype(jnp.int32) * jnp.arange(per_dev, dtype=jnp.int32)[None, :, None], axis=1
    )
    present = jnp.any(slot_hit, axis=1)
    request = jnp.where(present, local_ids, -1)
    asked = lax.all_to_all(request, "kv", split_axis=0, concat_axis=0, tiled=True)
    picked = jnp.clip(asked, 0).reshape(-1)
    send_keys = key_rows.reshape(per_dev, BLK, width)[picked]
    send_values = value_rows.reshape(per_dev, BLK, width)[picked]
    got_keys, got_values = (
        lax.all_to_all(send_keys, "kv", split_axis=0, concat_axis=0, tiled=True),
        lax.all_to_all(send_values, "kv", split_axis=0, concat_axis=0, tiled=True),
    )
    got_ids = jnp.where(present, peer_ids[:, None] * per_dev + local_ids, -1).reshape(-1)
    far_part = attend(
        query_rows,
        got_keys.reshape(-1, width),
        got_values.reshape(-1, width),
        got_ids,
        chosen,
        first_block,
    )
    merged = combine(own_part, far_part)
    normed = merged[2] / merged[1][..., None]
    attended = jnp.transpose(normed, (1, 0, 2)).reshape(tok_rows, width).astype(jnp.bfloat16)
    rows = attended
    return lax.psum_scatter(
        jnp.dot(rows, w_out, preferred_element_type=jnp.float32).astype(jnp.bfloat16),
        "tp",
        scatter_dimension=0,
        tiled=True,
    )


def solution(mesh):
    return jax.shard_map(
        local,
        mesh=mesh,
        in_specs=(
            P("kv", "tp"),
            P(None, "tp"),
            P(None, "tp"),
            P(None, "tp"),
            P("tp", None),
            P("kv", None),
        ),
        out_specs=P(("kv", "tp"), None),
        check_vma=False,
    )
```

profile of v0, /device:TPU:0, one launch (start us, length us, event | category | flops | bytes accessed | tf_op | source)
XLA Modules:
  0.0 118.5 jit_solution(13071488536581529827)
XLA Ops:
  7.3 0.8 fusion.26
  9.4 7.3 %all-to-all-start = ((s32[8,1,2]{2,1,0:T(1,128)}), s32[8,1,2]{2,1,0:T(1,128)S(1)}, u32[]{:S(2)}, u32[]{:S(2)}) async-start(s32[8,1,2]{2,1,0:T(1,128)} %copy.46), calls=%async_computation | async-start | bytes 8192 | tf_op jit(solution)/shard_map/all_to_all | solution.py:87
  16.9 1.4 %compare_reduce_fusion = (pred[16,16]{1,0:T(8,128)(4,1)S(1)}, pred[16,16]{1,0:T(8,128)(4,1)S(1)}) fusion(s32[16,24]{1,0:T(8,128)} %param.11, s32[16]{0:T(128)S(1)} %select_n.53, s32[16]{0:T(128)S(1)} %get-tuple-element.20), kind=kLoop, calls=%fused_computation.40 | loop fusion | flops 24064 | bytes 2176 | tf_op jit(solution)/shard_map/reduce_or | solution.py:19
  18.8 2.1 %reshape.338 = pred[512,512]{0,1:T(8,128)(4,1)S(1)} reshape(pred[16,32,16,32]{1,0,3,2:T(8,128)(4,1)S(1)} %broadcast_in_dim.42) | data formatting | bytes 524288 | tf_op jit(solution)/shard_map/reshape | solution.py:21
  21.5 2.1 %reshape.333 = pred[512,512]{0,1:T(8,128)(4,1)S(1)} reshape(pred[16,32,16,32]{1,0,3,2:T(8,128)(4,1)S(1)} %broadcast_in_dim.37) | data formatting | bytes 524288 | tf_op jit(solution)/shard_map/reshape | solution.py:21
  24.4 9.8 %all-gather.2.cloned.1.call-done = bf16[512,2048]{1,0:T(8,128)(2,1)} async-done(((bf16[512,512]{1,0:T(8,128)(2,1)}), bf16[512,2048]{1,0:T(8,128)(2,1)}) %all-gather.2.cloned.1.call-update) | async-done | bytes 2097168 | tf_op jit(solution)/shard_map/all_gather | solution.py:57
  34.2 3.3 %convolution_convert_fusion.1 = bf16[512,384]{1,0:T(8,128)(2,1)S(1)} fusion(bf16[512,2048]{1,0:T(8,128)(2,1)} %all-gather.2.cloned.1.call-done, bf16[2048,384]{1,0:T(8,128)(2,1)} %param.9), kind=kOutput, calls=%fused_computation.28 | convolution fusion | flops 805502976 | bytes 4063232 | tf_op jit(solution)/shard_map/dot_general | solution.py:61
  37.5 0.9 copy.42
  38.4 3.3 %convolution_convert_fusion.2 = bf16[512,384]{1,0:T(8,128)(2,1)S(1)} fusion(bf16[512,2048]{1,0:T(8,128)(2,1)} %all-gather.2.cloned.1.call-done, bf16[2048,384]{1,0:T(8,128)(2,1)} %param.8), kind=kOutput, calls=%fused_computation.29 | convolution fusion | flops 805502976 | bytes 4063232 | tf_op jit(solution)/shard_map/dot_general | solution.py:61
  41.9 1.3 %gather_fusion = bf16[16,32,384]{2,1,0:T(8,128)(2,1)} fusion(bf16[16,32,384]{2,1,0:T(8,128)(2,1)S(1)} %bitcast.62, s32[1024]{0:T(1024)S(1)} %pad_clamp_fusion), kind=kCustom, calls=%fused_computation | custom fusion | bytes 786496 | tf_op jit(solution)/shard_map/gather | solution.py:89
  43.3 5.5 %all-to-all-start.1 = ((bf16[16,32,384]{2,1,0:T(8,128)(2,1)}), bf16[16,32,384]{2,1,0:T(8,128)(2,1)S(1)}, u32[]{:S(2)}, u32[]{:S(2)}) async-start(bf16[16,32,384]{2,1,0:T(8,128)(2,1)} %gather_fusion), calls=%async_computation.1 | async-start | bytes 786432 | tf_op jit(solution)/shard_map/all_to_all | solution.py:92
  48.8 1.4 %gather_fusion.1 = bf16[16,32,384]{2,1,0:T(8,128)(2,1)} fusion(bf16[16,32,384]{2,1,0:T(8,128)(2,1)S(1)} %bitcast.61, s32[1024]{0:T(1024)S(1)} %pad_clamp_fusion), kind=kCustom, calls=%fused_computation.1 | custom fusion | bytes 786496 | tf_op jit(solution)/shard_map/gather | solution.py:90
  50.2 3.1 %convolution_convert_fusion.3 = bf16[512,384]{0,1:T(8,128)(2,1)S(1)} fusion(bf16[512,2048]{1,0:T(8,128)(2,1)} %all-gather.2.cloned.1.call-done, bf16[2048,384]{1,0:T(8,128)(2,1)} %param.7), kind=kOutput, calls=%fused_computation.30 | convolution fusion | flops 805502976 | bytes 4063232 | tf_op jit(solution)/shard_map/dot_general | solution.py:61
  54.1 1.7 %copy-done.1 = f32[3,512,512]{1,2,0:T(8,128)} copy-done((f32[3,512,512]{1,2,0:T(8,128)}, f32[3,512,512]{1,2,0:T(8,128)S(1)}, u32[]{:S(2)}) %copy-start.1) | copy-done | bytes 3145752
  55.7 0.8 fusion.2
  56.5 4.3 %all-to-all-done.1 = bf16[16,32,384]{2,1,0:T(8,128)(2,1)S(1)} async-done(((bf16[16,32,384]{2,1,0:T(8,128)(2,1)}), bf16[16,32,384]{2,1,0:T(8,128)(2,1)S(1)}, u32[]{:S(2)}, u32[]{:S(2)}) %all-to-all-start.1) | async-done | bytes 393248 | tf_op jit(solution)/shard_map/all_to_all | solution.py:92
  60.9 3.6 %all-to-all-start.2 = ((bf16[16,32,384]{2,1,0:T(8,128)(2,1)}), bf16[16,32,384]{2,1,0:T(8,128)(2,1)S(1)}, u32[]{:S(2)}, u32[]{:S(2)}) async-start(bf16[16,32,384]{2,1,0:T(8,128)(2,1)} %gather_fusion.1), calls=%async_computation.2 | async-start | bytes 786432 | tf_op jit(solution)/shard_map/all_to_all | solution.py:93
  64.9 1.9 %fusion.1 = (f32[3,512]{1,0:T(4,128)S(1)}, f32[3,512,512]{1,2,0:T(8,128)S(1)}) fusion(pred[512,512]{0,1:T(8,128)(4,1)S(1)} %get-tuple-element.12, bf16[512,3,128]{0,2,1:T(8,128)(2,1)} %bitcast.64, bf16[512,3,128]{2,1,0:T(4,128)(2,1)S(1)} %reshape_reshape.6), kind=kOutput, calls=%fused_computation.8 | convolution fusion | flops 203684352 | bytes 4200448 | tf_op jit(solution)/shard_map/qhd,khd->hqk/dot_general | solution.py:32
  66.8 1.7 %copy-done.3 = f32[3,512,512]{1,2,0:T(8,128)} copy-done((f32[3,512,512]{1,2,0:T(8,128)}, f32[3,512,512]{1,2,0:T(8,128)S(1)}, u32[]{:S(2)}) %copy-start.3) | copy-done | bytes 3145752
  69.3 1.9 %fusion.18 = f32[512,3,128]{0,2,1:T(8,128)} fusion(bf16[512,3,128]{0,2,1:T(8,128)(2,1)S(1)} %bitcast.65, f32[3,512,512]{1,2,0:T(8,128)S(1)} %copy-done.2, f32[3,512]{1,0:T(4,128)S(1)} %get-tuple-element.16, pred[512,512]{0,1:T(8,128)(4,1)S(1)} %get-tuple-element.13, f32[512,3]{0,1:T(4,128)S(1)} %get-tuple-element.9), kind=kOutput, calls=%fused_computation.25 | convolution fusion | flops 204668928 | bytes 4599808 | tf_op jit(solution)/shard_map/hqk,khd->hqd/dot_general | solution.py:39
  71.2 5.2 %all-to-all-done.2 = bf16[16,32,384]{2,1,0:T(8,128)(2,1)S(1)} async-done(((bf16[16,32,384]{2,1,0:T(8,128)(2,1)}), bf16[16,32,384]{2,1,0:T(8,128)(2,1)S(1)}, u32[]{:S(2)}, u32[]{:S(2)}) %all-to-all-start.2) | async-done | bytes 393248 | tf_op jit(solution)/shard_map/all_to_all | solution.py:93
  76.5 3.1 %fusion.22 = bf16[512,3,128]{0,2,1:T(8,128)(2,1)S(1)} fusion(f32[512,3,128]{0,2,1:T(8,128)} %fusion.18, f32[3,512,512]{1,2,0:T(8,128)} %copy-done.3, f32[3,512]{1,0:T(4,128)S(1)} %get-tuple-element.18, pred[512,512]{0,1:T(8,128)(4,1)S(1)} %get-tuple-element.12, bf16[512,3,128]{2,1,0:T(4,128)(2,1)S(1)} %reshape_reshape.7, ...), kind=kOutput, calls=%fused_computation.34 | convolution fusion | flops 205258752 | bytes 4999168 | tf_op jit(solution)/shard_map/hqk,khd->hqd/dot_general | solution.py:39
  79.6 2.7 %convolution_convert_fusion = bf16[512,2048]{1,0:T(8,128)(2,1)} fusion(bf16[512,384]{0,1:T(8,128)(2,1)S(1)} %bitcast.66, bf16[384,2048]{1,0:T(8,128)(2,1)S(1)} %copy-done), kind=kOutput, calls=%fused_computation.6 | convolution fusion | flops 806354944 | bytes 4063232 | tf_op jit(solution)/shard_map/dot_general | solution.py:109
  82.3 29.4 %reduce-scatter.2.cloned.1.call-done = bf16[128,2048]{1,0:T(8,128)(2,1)} async-done(((bf16[512,2048]{1,0:T(8,128)(2,1)}), bf16[128,2048]{1,0:T(8,128)(2,1)}) %reduce-scatter.2.cloned.1.call-update) | async-done | bytes 524304 | tf_op jit(solution)/shard_map/reduce_scatter | solution.py:108
  (52 shorter events, 6.3 us)
Async XLA Ops:
  6.5 73.0 %copy-start = (bf16[384,2048]{1,0:T(8,128)(2,1)S(1)}, bf16[384,2048]{1,0:T(8,128)(2,1)}, u32[]{:S(2)}) copy-start(bf16[384,2048]{1,0:T(8,128)(2,1)} %param.10) | copy-start | bytes 4718596
  6.5 27.7 %all-gather.2.cloned.1.call-start = ((), (), s32[]{:S(2)}) async-start(), calls=%async_computation.4 | async-start | bytes 2621440 | tf_op jit(solution)/shard_map/all_gather | solution.py:57
  9.4 14.8 %all-to-all-start = ((s32[8,1,2]{2,1,0:T(1,128)}), s32[8,1,2]{2,1,0:T(1,128)S(1)}, u32[]{:S(2)}, u32[]{:S(2)}) async-start(s32[8,1,2]{2,1,0:T(1,128)} %copy.46), calls=%async_computation | async-start | bytes 8192 | tf_op jit(solution)/shard_map/all_to_all | solution.py:87
  43.3 17.6 %all-to-all-start.1 = ((bf16[16,32,384]{2,1,0:T(8,128)(2,1)}), bf16[16,32,384]{2,1,0:T(8,128)(2,1)S(1)}, u32[]{:S(2)}, u32[]{:S(2)}) async-start(bf16[16,32,384]{2,1,0:T(8,128)(2,1)} %gather_fusion), calls=%async_computation.1 | async-start | bytes 786432 | tf_op jit(solution)/shard_map/all_to_all | solution.py:92
  53.2 11.3 %copy-start.4 = (bf16[512,384]{0,1:T(8,128)(2,1)}, bf16[512,384]{0,1:T(8,128)(2,1)S(1)}, u32[]{:S(2)}) copy-start(bf16[512,384]{0,1:T(8,128)(2,1)S(1)} %convolution_convert_fusion.3) | copy-start | bytes 1179652
  54.0 1.7 %copy-start.1 = (f32[3,512,512]{1,2,0:T(8,128)}, f32[3,512,512]{1,2,0:T(8,128)S(1)}, u32[]{:S(2)}) copy-start(f32[3,512,512]{1,2,0:T(8,128)S(1)} %get-tuple-element.17) | copy-start | bytes 9437188
  60.9 15.5 %all-to-all-start.2 = ((bf16[16,32,384]{2,1,0:T(8,128)(2,1)}), bf16[16,32,384]{2,1,0:T(8,128)(2,1)S(1)}, u32[]{:S(2)}, u32[]{:S(2)}) async-start(bf16[16,32,384]{2,1,0:T(8,128)(2,1)} %gather_fusion.1), calls=%async_computation.2 | async-start | bytes 786432 | tf_op jit(solution)/shard_map/all_to_all | solution.py:93
  64.5 47.2 %reduce-scatter.2.cloned.1.call-start = ((), (), s32[]{:S(2)}) async-start(), calls=%async_computation.5 | async-start | bytes 2621440 | tf_op jit(solution)/shard_map/reduce_scatter | solution.py:108
  64.8 4.5 %copy-start.2 = (f32[3,512,512]{1,2,0:T(8,128)S(1)}, f32[3,512,512]{1,2,0:T(8,128)}, u32[]{:S(2)}) copy-start(f32[3,512,512]{1,2,0:T(8,128)} %copy-done.1) | copy-start | bytes 9437188
  64.9 4.5 %copy-start.5 = (bf16[512,384]{0,1:T(8,128)(2,1)S(1)}, bf16[512,384]{0,1:T(8,128)(2,1)}, u32[]{:S(2)}) copy-start(bf16[512,384]{0,1:T(8,128)(2,1)} %copy.42) | copy-start | bytes 1179652
  66.8 1.7 %copy-start.3 = (f32[3,512,512]{1,2,0:T(8,128)}, f32[3,512,512]{1,2,0:T(8,128)S(1)}, u32[]{:S(2)}) copy-start(f32[3,512,512]{1,2,0:T(8,128)S(1)} %get-tuple-element.19) | copy-start | bytes 9437188
Sparse Core Ops, SparseCore 0:
  8.9 25.2 all-gather.1
  82.4 29.2 reduce-scatter.1
where the time goes:
time: 119 us
  waiting for transfers between devices  49.5 us (42%)
  matrix products  19.9 us (17%)
  starting transfers between devices  16.7 us (14%)
  local copies, waits for them, and re-layouts  13.7 us (12%)
  between operations  13.6 us (11%)
  other arithmetic  5.12 us (4%)
    reduce_scatter x1, waiting for transfers between devices, local(): lax.psum_scatter(jnp.dot(rows, w_out, preferred_element_type=jnp.float32)...  29.4 us
    all_gather x1, waiting for transfers between devices, local(): piece = lax.all_gather(tokens, 'tp', axis=1, tiled=True)  9.83 us
    dot_general x3, matrix products, local(): outputs.append(jnp.dot(piece, rows, preferred_element_type=jnp.float32))  9.62 us
    all_to_all x1, starting transfers between devices, local(): lax.all_to_all(request, 'kv', split_axis=0, concat_axis=0, tiled=True)  7.31 us
    all_to_all x1, starting transfers between devices, local(): lax.all_to_all(send_keys, 'kv', split_axis=0, concat_axis=0, tiled=True)  5.51 us
    all_to_all x1, waiting for transfers between devices, local(): lax.all_to_all(send_values, 'kv', split_axis=0, concat_axis=0, tiled=True)  5.16 us
    dot_general x2, matrix products, attend(): jnp.einsum('hqk,khd->hqd', weights, value_heads.astype(jnp.float32))  4.96 us
    all_to_all x1, waiting for transfers between devices, local(): lax.all_to_all(send_keys, 'kv', split_axis=0, concat_axis=0, tiled=True)  4.32 us
  transfers between devices with their start and end apart: 5, of which 4 were waited for; matrix products, arithmetic and copies ran while one was open for 17% of the time, Pallas kernels for 0%

commit v1 on v0

--- a/solution.py
+++ b/solution.py
@@ -54,7 +54,7 @@
     width = w_query.shape[1]
     empty = jnp.zeros((tok_rows, width), jnp.float32)
     totals = (empty, empty, empty)
-    piece = lax.all_gather(tokens, "tp", axis=1, tiled=True)
+    piece = jnp.concatenate(lax.all_gather(tokens, "tp"), axis=1)
     outputs = []
     for total, weight in zip(totals, (w_query, w_key, w_value)):
         rows = weight

time: 119 us -> 125 us (1.050)
  local copies, waits for them, and re-layouts: 13.7 us -> 17.8 us
  waiting for transfers between devices: 49.5 us -> 51.5 us
    reshape x0 -> x1, local copies, waits for them, and re-layouts: none -> 4.14 us  [local(): piece = jnp.concatenate(lax.all_gather(tokens, 'tp'), axis=1)]
    all_to_all x1, waiting for transfers between devices: 4.32 us -> 6.4 us  [local(): lax.all_to_all(send_keys, 'kv', split_axis=0, concat_axis=0, tiled=True)]
    unnamed x12 -> x14, local copies, waits for them, and re-layouts: 3.37 us -> 3.38 us
  transfers between devices with their start and end apart: 5 -> 5, of which waited for: 4 -> 4; matrix products, arithmetic and copies ran while one was open for 17% -> 15% of each run, Pallas kernels for 0% -> 0%
where the time goes in v1:
time: 125 us
  waiting for transfers between devices  51.5 us (41%)
  matrix products  19.9 us (16%)
  local copies, waits for them, and re-layouts  17.8 us (14%)
  starting transfers between devices  16.7 us (13%)
  between operations  13.6 us (11%)
  other arithmetic  5.12 us (4%)
    reduce_scatter x1, waiting for transfers between devices, local(): lax.psum_scatter(jnp.dot(rows, w_out, preferred_element_type=jnp.float32)...  29.4 us
    all_gather x1, waiting for transfers between devices, local(): piece = jnp.concatenate(lax.all_gather(tokens, 'tp'), axis=1)  9.82 us
    dot_general x3, matrix products, local(): outputs.append(jnp.dot(piece, rows, preferred_element_type=jnp.float32))  8.55 us
    all_to_all x1, starting transfers between devices, local(): lax.all_to_all(request, 'kv', split_axis=0, concat_axis=0, tiled=True)  7.31 us
    all_to_all x1, waiting for transfers between devices, local(): lax.all_to_all(send_keys, 'kv', split_axis=0, concat_axis=0, tiled=True)  6.4 us
    all_to_all x1, starting transfers between devices, local(): lax.all_to_all(send_keys, 'kv', split_axis=0, concat_axis=0, tiled=True)  5.51 us
    all_to_all x1, waiting for transfers between devices, local(): lax.all_to_all(send_values, 'kv', split_axis=0, concat_axis=0, tiled=True)  5.17 us
    dot_general x2, matrix products, attend(): jnp.einsum('hqk,khd->hqd', weights, value_heads.astype(jnp.float32))  4.95 us
  transfers between devices with their start and end apart: 5, of which 4 were waited for; matrix products, arithmetic and copies ran while one was open for 15% of the time, Pallas kernels for 0%

profile of v1, /device:TPU:0, one launch (start us, length us, event | category | flops | bytes accessed | tf_op | source)
XLA Modules:
  0.0 124.6 jit_solution(4643638261088283786)
XLA Ops:
  9.4 7.3 %all-to-all-start = ((s32[8,1,2]{2,1,0:T(1,128)}), s32[8,1,2]{2,1,0:T(1,128)S(1)}, u32[]{:S(2)}, u32[]{:S(2)}) async-start(s32[8,1,2]{2,1,0:T(1,128)} %copy.60), calls=%async_computation | async-start | bytes 8192 | tf_op jit(solution)/shard_map/all_to_all | solution.py:87
  16.9 1.4 %compare_reduce_fusion = (pred[16,16]{1,0:T(8,128)(4,1)S(1)}, pred[16,16]{1,0:T(8,128)(4,1)S(1)}) fusion(s32[16,24]{1,0:T(8,128)} %param.11, s32[16]{0:T(128)S(1)} %select_n.53, s32[16]{0:T(128)S(1)} %get-tuple-element.20), kind=kLoop, calls=%fused_computation.40 | loop fusion | flops 24064 | bytes 2176 | tf_op jit(solution)/shard_map/reduce_or | solution.py:19
  18.8 2.1 %reshape.346 = pred[512,512]{0,1:T(8,128)(4,1)S(1)} reshape(pred[16,32,16,32]{1,0,3,2:T(8,128)(4,1)S(1)} %broadcast_in_dim.42) | data formatting | bytes 524288 | tf_op jit(solution)/shard_map/reshape | solution.py:21
  21.5 2.1 %reshape.339 = pred[512,512]{0,1:T(8,128)(4,1)S(1)} reshape(pred[16,32,16,32]{1,0,3,2:T(8,128)(4,1)S(1)} %broadcast_in_dim.37) | data formatting | bytes 524288 | tf_op jit(solution)/shard_map/reshape | solution.py:21
  24.4 9.8 %all-gather.3.cloned.1.call-done = bf16[2048,512]{1,0:T(8,128)(2,1)} async-done(((bf16[512,512]{1,0:T(8,128)(2,1)}), bf16[2048,512]{1,0:T(8,128)(2,1)}) %all-gather.3.cloned.1.call-update) | async-done | bytes 2097168 | tf_op jit(solution)/shard_map/all_gather | solution.py:57
  34.2 4.1 %copy.52 = bf16[512,4,512]{0,2,1:T(8,128)(2,1)} copy(bf16[512,4,512]{2,0,1:T(8,128)(2,1)} %bitcast.69) | data formatting | bytes 4194304 | tf_op jit(solution)/shard_map/reshape | solution.py:57
  38.4 3.3 %convolution_convert_fusion.1 = bf16[512,384]{1,0:T(8,128)(2,1)S(1)} fusion(bf16[512,2048]{0,1:T(8,128)(2,1)} %bitcast.64, bf16[2048,384]{1,0:T(8,128)(2,1)} %param.9), kind=kOutput, calls=%fused_computation.28 | convolution fusion | flops 805502976 | bytes 4063232 | tf_op jit(solution)/shard_map/dot_general | solution.py:61
  41.7 0.9 copy.56
  42.6 4.0 %convolution_convert_fusion.3 = bf16[512,384]{0,1:T(8,128)(2,1)} fusion(bf16[512,2048]{0,1:T(8,128)(2,1)} %bitcast.65, bf16[2048,384]{1,0:T(8,128)(2,1)} %param.7), kind=kOutput, calls=%fused_computation.30 | convolution fusion | flops 805502976 | bytes 4063232 | tf_op jit(solution)/shard_map/dot_general | solution.py:61
  46.6 1.3 %convolution_convert_fusion.2 = bf16[512,384]{1,0:T(8,128)(2,1)S(1)} fusion(bf16[512,2048]{0,1:T(8,128)(2,1)S(1)} %bitcast.66, bf16[2048,384]{1,0:T(8,128)(2,1)S(1)} %copy-done.5), kind=kOutput, calls=%fused_computation.29 | convolution fusion | flops 805502976 | bytes 4063232 | tf_op jit(solution)/shard_map/dot_general | solution.py:61
  48.1 1.3 %gather_fusion = bf16[16,32,384]{2,1,0:T(8,128)(2,1)} fusion(bf16[16,32,384]{2,1,0:T(8,128)(2,1)S(1)} %bitcast.68, s32[1024]{0:T(1024)S(1)} %pad_clamp_fusion), kind=kCustom, calls=%fused_computation | custom fusion | bytes 786496 | tf_op jit(solution)/shard_map/gather | solution.py:89
  49.4 5.5 %all-to-all-start.1 = ((bf16[16,32,384]{2,1,0:T(8,128)(2,1)}), bf16[16,32,384]{2,1,0:T(8,128)(2,1)S(1)}, u32[]{:S(2)}, u32[]{:S(2)}) async-start(bf16[16,32,384]{2,1,0:T(8,128)(2,1)} %gather_fusion), calls=%async_computation.1 | async-start | bytes 786432 | tf_op jit(solution)/shard_map/all_to_all | solution.py:92
  54.9 1.4 %gather_fusion.1 = bf16[16,32,384]{2,1,0:T(8,128)(2,1)} fusion(bf16[16,32,384]{2,1,0:T(8,128)(2,1)S(1)} %bitcast.67, s32[1024]{0:T(1024)S(1)} %pad_clamp_fusion), kind=kCustom, calls=%fused_computation.1 | custom fusion | bytes 786496 | tf_op jit(solution)/shard_map/gather | solution.py:90
  56.3 1.8 %fusion = (f32[3,512]{1,0:T(4,128)S(1)}, f32[3,512,512]{1,2,0:T(8,128)S(1)}) fusion(pred[512,512]{0,1:T(8,128)(4,1)S(1)} %get-tuple-element.13, bf16[512,3,128]{0,2,1:T(8,128)(2,1)} %bitcast.71, bf16[512,3,128]{0,2,1:T(8,128)(2,1)S(1)} %bitcast.70), kind=kOutput, calls=%fused_computation.7 | convolution fusion | flops 203684352 | bytes 4200448 | tf_op jit(solution)/shard_map/qhd,khd->hqk/dot_general | solution.py:32
  58.1 1.7 %copy-done.2 = f32[3,512,512]{1,2,0:T(8,128)} copy-done((f32[3,512,512]{1,2,0:T(8,128)}, f32[3,512,512]{1,2,0:T(8,128)S(1)}, u32[]{:S(2)}) %copy-start.2) | copy-done | bytes 3145752
  60.6 6.4 %all-to-all-done.1 = bf16[16,32,384]{2,1,0:T(8,128)(2,1)S(1)} async-done(((bf16[16,32,384]{2,1,0:T(8,128)(2,1)}), bf16[16,32,384]{2,1,0:T(8,128)(2,1)S(1)}, u32[]{:S(2)}, u32[]{:S(2)}) %all-to-all-start.1) | async-done | bytes 393248 | tf_op jit(solution)/shard_map/all_to_all | solution.py:92
  67.0 3.6 %all-to-all-start.2 = ((bf16[16,32,384]{2,1,0:T(8,128)(2,1)}), bf16[16,32,384]{2,1,0:T(8,128)(2,1)S(1)}, u32[]{:S(2)}, u32[]{:S(2)}) async-start(bf16[16,32,384]{2,1,0:T(8,128)(2,1)} %gather_fusion.1), calls=%async_computation.2 | async-start | bytes 786432 | tf_op jit(solution)/shard_map/all_to_all | solution.py:93
  71.0 1.9 %fusion.1 = (f32[3,512]{1,0:T(4,128)S(1)}, f32[3,512,512]{1,2,0:T(8,128)S(1)}) fusion(pred[512,512]{0,1:T(8,128)(4,1)S(1)} %get-tuple-element.12, bf16[512,3,128]{0,2,1:T(8,128)(2,1)} %bitcast.72, bf16[512,3,128]{2,1,0:T(4,128)(2,1)S(1)} %reshape_reshape.6), kind=kOutput, calls=%fused_computation.8 | convolution fusion | flops 203684352 | bytes 4200448 | tf_op jit(solution)/shard_map/qhd,khd->hqk/dot_general | solution.py:32
  72.9 1.7 %copy-done.4 = f32[3,512,512]{1,2,0:T(8,128)} copy-done((f32[3,512,512]{1,2,0:T(8,128)}, f32[3,512,512]{1,2,0:T(8,128)S(1)}, u32[]{:S(2)}) %copy-start.4) | copy-done | bytes 3145752
  75.4 1.9 %fusion.18 = f32[512,3,128]{0,2,1:T(8,128)} fusion(bf16[512,3,128]{0,2,1:T(8,128)(2,1)S(1)} %bitcast.73, f32[3,512,512]{1,2,0:T(8,128)S(1)} %copy-done.3, f32[3,512]{1,0:T(4,128)S(1)} %get-tuple-element.16, pred[512,512]{0,1:T(8,128)(4,1)S(1)} %get-tuple-element.13, f32[512,3]{0,1:T(4,128)S(1)} %get-tuple-element.9), kind=kOutput, calls=%fused_computation.25 | convolution fusion | flops 204668928 | bytes 4599808 | tf_op jit(solution)/shard_map/hqk,khd->hqd/dot_general | solution.py:39
  77.3 5.2 %all-to-all-done.2 = bf16[16,32,384]{2,1,0:T(8,128)(2,1)S(1)} async-done(((bf16[16,32,384]{2,1,0:T(8,128)(2,1)}), bf16[16,32,384]{2,1,0:T(8,128)(2,1)S(1)}, u32[]{:S(2)}, u32[]{:S(2)}) %all-to-all-start.2) | async-done | bytes 393248 | tf_op jit(solution)/shard_map/all_to_all | solution.py:93
  82.6 3.1 %fusion.22 = bf16[512,3,128]{0,2,1:T(8,128)(2,1)S(1)} fusion(f32[512,3,128]{0,2,1:T(8,128)} %fusion.18, f32[3,512,512]{1,2,0:T(8,128)} %copy-done.4, f32[3,512]{1,0:T(4,128)S(1)} %get-tuple-element.18, pred[512,512]{0,1:T(8,128)(4,1)S(1)} %get-tuple-element.12, bf16[512,3,128]{2,1,0:T(4,128)(2,1)S(1)} %reshape_reshape.7, ...), kind=kOutput, calls=%fused_computation.34 | convolution fusion | flops 205258752 | bytes 4999168 | tf_op jit(solution)/shard_map/hqk,khd->hqd/dot_general | solution.py:39
  85.7 2.7 %convolution_convert_fusion = bf16[512,2048]{1,0:T(8,128)(2,1)} fusion(bf16[512,384]{0,1:T(8,128)(2,1)S(1)} %bitcast.74, bf16[384,2048]{1,0:T(8,128)(2,1)S(1)} %copy-done), kind=kOutput, calls=%fused_computation.6 | convolution fusion | flops 806354944 | bytes 4063232 | tf_op jit(solution)/shard_map/dot_general | solution.py:109
  88.4 29.4 %reduce-scatter.2.cloned.1.call-done = bf16[128,2048]{1,0:T(8,128)(2,1)} async-done(((bf16[512,2048]{1,0:T(8,128)(2,1)}), bf16[128,2048]{1,0:T(8,128)(2,1)}) %reduce-scatter.2.cloned.1.call-update) | async-done | bytes 524304 | tf_op jit(solution)/shard_map/reduce_scatter | solution.py:108
  (55 shorter events, 7.1 us)
Async XLA Ops:
  6.5 79.2 %copy-start = (bf16[384,2048]{1,0:T(8,128)(2,1)S(1)}, bf16[384,2048]{1,0:T(8,128)(2,1)}, u32[]{:S(2)}) copy-start(bf16[384,2048]{1,0:T(8,128)(2,1)} %param.10) | copy-start | bytes 4718596
  6.5 27.7 %all-gather.3.cloned.1.call-start = ((), (), s32[]{:S(2)}) async-start(), calls=%async_computation.5 | async-start | bytes 2621440 | tf_op jit(solution)/shard_map/all_gather | solution.py:57
  9.4 14.8 %all-to-all-start = ((s32[8,1,2]{2,1,0:T(1,128)}), s32[8,1,2]{2,1,0:T(1,128)S(1)}, u32[]{:S(2)}, u32[]{:S(2)}) async-start(s32[8,1,2]{2,1,0:T(1,128)} %copy.60), calls=%async_computation | async-start | bytes 8192 | tf_op jit(solution)/shard_map/all_to_all | solution.py:87
  42.6 4.0 %copy-start.1 = (bf16[512,4,512]{0,2,1:T(8,128)(2,1)S(1)}, bf16[512,4,512]{0,2,1:T(8,128)(2,1)}, u32[]{:S(2)}) copy-start(bf16[512,4,512]{0,2,1:T(8,128)(2,1)} %copy.52) | copy-start | bytes 6291460
  42.6 4.0 %copy-start.5 = (bf16[2048,384]{1,0:T(8,128)(2,1)S(1)}, bf16[2048,384]{1,0:T(8,128)(2,1)}, u32[]{:S(2)}) copy-start(bf16[2048,384]{1,0:T(8,128)(2,1)} %param.8) | copy-start | bytes 4718596
  49.4 17.6 %all-to-all-start.1 = ((bf16[16,32,384]{2,1,0:T(8,128)(2,1)}), bf16[16,32,384]{2,1,0:T(8,128)(2,1)S(1)}, u32[]{:S(2)}, u32[]{:S(2)}) async-start(bf16[16,32,384]{2,1,0:T(8,128)(2,1)} %gather_fusion), calls=%async_computation.1 | async-start | bytes 786432 | tf_op jit(solution)/shard_map/all_to_all | solution.py:92
  58.1 1.7 %copy-start.2 = (f32[3,512,512]{1,2,0:T(8,128)}, f32[3,512,512]{1,2,0:T(8,128)S(1)}, u32[]{:S(2)}) copy-start(f32[3,512,512]{1,2,0:T(8,128)S(1)} %get-tuple-element.17) | copy-start | bytes 9437188
  67.0 15.5 %all-to-all-start.2 = ((bf16[16,32,384]{2,1,0:T(8,128)(2,1)}), bf16[16,32,384]{2,1,0:T(8,128)(2,1)S(1)}, u32[]{:S(2)}, u32[]{:S(2)}) async-start(bf16[16,32,384]{2,1,0:T(8,128)(2,1)} %gather_fusion.1), calls=%async_computation.2 | async-start | bytes 786432 | tf_op jit(solution)/shard_map/all_to_all | solution.py:93
  70.6 47.2 %reduce-scatter.2.cloned.1.call-start = ((), (), s32[]{:S(2)}) async-start(), calls=%async_computation.4 | async-start | bytes 2621440 | tf_op jit(solution)/shard_map/reduce_scatter | solution.py:108
  71.0 4.5 %copy-start.3 = (f32[3,512,512]{1,2,0:T(8,128)S(1)}, f32[3,512,512]{1,2,0:T(8,128)}, u32[]{:S(2)}) copy-start(f32[3,512,512]{1,2,0:T(8,128)} %copy-done.2) | copy-start | bytes 9437188
  71.0 4.5 %copy-start.6 = (bf16[512,384]{0,1:T(8,128)(2,1)S(1)}, bf16[512,384]{0,1:T(8,128)(2,1)}, u32[]{:S(2)}) copy-start(bf16[512,384]{0,1:T(8,128)(2,1)} %copy.56) | copy-start | bytes 1179652
  72.9 1.7 %copy-start.4 = (f32[3,512,512]{1,2,0:T(8,128)}, f32[3,512,512]{1,2,0:T(8,128)S(1)}, u32[]{:S(2)}) copy-start(f32[3,512,512]{1,2,0:T(8,128)S(1)} %get-tuple-element.19) | copy-start | bytes 9437188
Sparse Core Ops, SparseCore 0:
  8.9 25.2 all-gather.2
  88.5 29.2 reduce-scatter.1
